TPU v7x, 128 devices: a whole 4x4x4 slice. The times are simulated.
128 devices in a mesh: fs: 16 (over z, x), tp: 8 (over y, core).
Axes of the slice: x: 4, y: 4, z: 4, core: 2. Of those that a mesh axis runs over, the one named last changes fastest.
Arguments:
- later_input: bfloat16 [12288, 2048], P('fs', 'tp'), may hold values from -6 to 6
- earlier_input: bfloat16 [12288, 2048], P('fs', 'tp'), may hold values from -6 to 6
- cotangent: bfloat16 [12288, 2048], P('fs', 'tp'), may hold values from -6 to 6
- up_weight: bfloat16 [2048, 8192], P('fs', 'tp'), may hold values from -0.125 to 0.125
- down_weight: bfloat16 [8192, 2048], P('tp', 'fs'), may hold values from -0.0625 to 0.0625
- up_running: float32 [2048, 8192], P('fs', 'tp'), may hold values from -6 to 6
- down_running: float32 [2048, 8192], P('fs', 'tp'), may hold values from -6 to 6
Outputs:
- later_output: bfloat16 [12288, 2048], P('fs', 'tp')
- later_preact: bfloat16 [12288, 8192], P('fs', 'tp')
- earlier_grad: bfloat16 [12288, 2048], P('fs', 'tp')
- up_running_out: float32 [2048, 8192], P('fs', 'tp')
- down_running_out: float32 [2048, 8192], P('fs', 'tp')
All inputs are finite; a program needn't handle non-finite values.
Results may differ from a plain program's by a relative error of at most 0.014.
Values may be sent and summed in bfloat16 or wider, within the bound.
A program may use at most 128 MiB of HBM per device.

v0:
```python
import jax
import jax.numpy as jnp
from jax import lax
from jax.sharding import PartitionSpec as P

contract_last = (((1,), (1,)), ((), ()))
contract_first = (((0,), (0,)), ((), ()))


def in_one_piece(arrays, axis, dim, along):
    ends, at = ([], 0)
    for a in arrays[:-1]:
        at += a.shape[along]
        ends.append(at)
    both = jnp.concatenate(arrays, axis=along)
    return tuple(jnp.split(lax.all_gather(both, axis, axis=dim, tiled=True), ends, axis=along))


def gather_turned(arrays, axis, dims):
    turned = [jnp.moveaxis(a, dim, 0) for a, dim in zip(arrays, dims)]
    widths = [t[0].size for t in turned]
    both = jnp.concatenate([t.reshape(-1, w) for t, w in zip(turned, widths)], axis=1)
    filled = lax.all_gather(both, axis, axis=0, tiled=True)
    tiles = jnp.split(filled, [sum(widths[:k]) for k in range(1, len(widths))], axis=1)
    return tuple(
        (
            jnp.moveaxis(b.reshape(-1, *t.shape[1:]), 0, dim)
            for b, t, dim in zip(tiles, turned, dims)
        )
    )


def side_by_side(arrays, axis, dim, along):
    both = jnp.concatenate(arrays, axis=along)
    filled, at, outs = (lax.psum_scatter(both, axis, scatter_dimension=dim, tiled=True), 0, [])
    for a in arrays:
        outs.append(lax.slice_in_dim(filled, at, at + a.shape[along], axis=along))
        at += a.shape[along]
    return tuple(outs)


def on_device(
    later_input, earlier_input, cotangent, up_weight, down_weight, up_running, down_running
):
    rows = later_input.shape[0]
    factor = float(rows * lax.axis_size("fs")) ** (-0.5)
    later_full, earlier_full, cot_full = in_one_piece(
        (later_input, earlier_input, cotangent), "tp", 1, 0
    )
    columns = up_weight.shape[1]
    up_whole, down_whole = gather_turned((up_weight, down_weight), "fs", (0, 1))
    later_up = jnp.dot(later_full, up_whole, preferred_element_type=jnp.float32)
    earlier_up = jnp.dot(earlier_full, up_whole, preferred_element_type=jnp.float32)
    later_hidden = jnp.square(jax.nn.relu(later_up)).astype(jnp.bfloat16)
    out_part = jnp.dot(later_hidden, down_whole, preferred_element_type=jnp.float32)
    hidden_grad = lax.dot_general(
        cot_full, down_whole, contract_last, preferred_element_type=jnp.float32
    )
    up_grad = (2.0 * jax.nn.relu(earlier_up) * hidden_grad).astype(jnp.bfloat16)
    back_part = lax.dot_general(
        up_grad, up_whole, contract_last, preferred_element_type=jnp.float32
    )
    later_preact = later_up.astype(jnp.bfloat16)
    earlier_hidden = jnp.square(jax.nn.relu(earlier_up)).astype(jnp.bfloat16)
    out_sum, back_sum = tuple(
        (
            part.astype(jnp.float32)
            for part in side_by_side(
                (out_part.astype(jnp.bfloat16), back_part.astype(jnp.bfloat16)), "tp", 1, 0
            )
        )
    )
    summed = lax.psum_scatter(
        jnp.concatenate(
            (
                lax.dot_general(
                    earlier_full, up_grad, contract_first, preferred_element_type=jnp.float32
                ),
                lax.dot_general(
                    cot_full, earlier_hidden, contract_first, preferred_element_type=jnp.float32
                ),
            ),
            axis=1,
        ).astype(jnp.bfloat16),
        "fs",
        scatter_dimension=0,
        tiled=True,
    ).astype(jnp.float32)
    grad_up_sum = summed[:, :columns]
    grad_down_sum = summed[:, columns:]
    return (
        out_sum.astype(jnp.bfloat16),
        later_preact,
        back_sum.astype(jnp.bfloat16),
        up_running + grad_up_sum * factor,
        down_running + grad_down_sum * factor,
    )


def solution(mesh):
    in_specs = (
        P("fs", "tp"),
        P("fs", "tp"),
        P("fs", "tp"),
        P("fs", "tp"),
        P("tp", "fs"),
        P("fs", "tp"),
        P("fs", "tp"),
    )
    out_specs = (P("fs", "tp"), P("fs", "tp"), P("fs", "tp"), P("fs", "tp"), P("fs", "tp"))
    return jax.shard_map(
        on_device, mesh=mesh, in_specs=in_specs, out_specs=out_specs, check_vma=False
    )
```

profile of v0, /device:TPU:0, one launch (start us, length us, event | category | flops | bytes accessed | tf_op | source)
XLA Modules:
  0.0 322.6 jit_solution(7393562719880853422)
XLA Ops:
  7.2 1.1 copy.17
  8.3 1.8 pad_maximum_fusion.3
  10.2 2.3 pad_maximum_fusion.2
  12.6 77.9 %all-gather.5.cloned.1.call-done = bf16[2048,2048]{0,1:T(8,128)(2,1)} async-done(((bf16[128,2048]{0,1:T(8,128)(2,1)}), bf16[2048,2048]{0,1:T(8,128)(2,1)}) %all-gather.5.cloned.1.call-update) | async-done | bytes 8388624 | tf_op jit(solution)/shard_map/all_gather | solution.py:23
  90.5 59.5 %all-gather.3.cloned.1.call-done = bf16[2304,2048]{1,0:T(8,128)(2,1)} async-done(((bf16[2304,256]{1,0:T(8,128)(2,1)}), bf16[2304,2048]{1,0:T(8,128)(2,1)}) %all-gather.3.cloned.1.call-update) | async-done | bytes 9437200 | tf_op jit(solution)/shard_map/all_gather | solution.py:16
  150.0 6.3 %fusion.8 = f32[768,1024]{1,0:T(8,128)S(1)} fusion(bf16[2048,2048]{0,1:T(8,128)(2,1)} %all-gather.5.cloned.1.call-done, bf16[2304,2048]{1,0:T(8,128)(2,1)} %all-gather.3.cloned.1.call-done), kind=kOutput, calls=%fused_computation.11 | convolution fusion | flops 3221225472 | bytes 10485760 | tf_op jit(solution)/shard_map/dot_general | solution.py:53
  156.4 1.9 copy-done.3
  158.3 4.7 %fusion.28 = (bf16[768,1024]{1,0:T(8,128)(2,1)}, f32[768,1024]{1,0:T(8,128)S(1)}) fusion(bf16[2048,2048]{0,1:T(8,128)(2,1)S(1)} %copy-done.3, bf16[2304,2048]{1,0:T(8,128)(2,1)S(1)} %copy-done.2), kind=kOutput, calls=%fused_computation.34 | convolution fusion | flops 3222011904 | bytes 12058624 | tf_op jit(solution)/shard_map/dot_general | solution.py:52
  163.0 3.6 %multiply_convert_fusion.1 = bf16[768,1024]{1,0:T(8,128)(2,1)S(1)} fusion(f32[768,1024]{1,0:T(8,128)S(1)} %fusion.8, bf16[2048,2048]{0,1:T(8,128)(2,1)S(1)} %copy-done.3, bf16[2304,2048]{1,0:T(8,128)(2,1)S(1)} %copy-done.2), kind=kOutput, calls=%fused_computation.17 | convolution fusion | flops 3224371200 | bytes 12058624 | tf_op jit(solution)/shard_map/dot_general | solution.py:56
  166.6 3.7 %convolution_convert_fusion.2 = bf16[768,2048]{1,0:T(8,128)(2,1)S(1)} fusion(bf16[768,1024]{1,0:T(8,128)(2,1)S(1)} %multiply_convert_fusion.1, bf16[2048,2048]{0,1:T(8,128)(2,1)S(1)} %copy-done.3), kind=kOutput, calls=%fused_computation.9 | convolution fusion | flops 3222798336 | bytes 8912896 | tf_op jit(solution)/shard_map/dot_general | solution.py:60
  170.2 5.9 %fusion.4 = bf16[768,2048]{1,0:T(8,128)(2,1)S(1)} fusion(bf16[2048,2048]{0,1:T(8,128)(2,1)} %all-gather.5.cloned.1.call-done, f32[768,1024]{1,0:T(8,128)S(1)} %get-tuple-element.20), kind=kOutput, calls=%fused_computation.8 | convolution fusion | flops 3225157632 | bytes 10485760 | tf_op jit(solution)/shard_map/dot_general | solution.py:55
  176.1 3.8 %pad_maximum_fusion.1 = bf16[1536,2048]{1,0:T(8,128)(2,1)} fusion(bf16[768,2048]{1,0:T(8,128)(2,1)S(1)} %convolution_convert_fusion.2, bf16[768,2048]{1,0:T(8,128)(2,1)S(1)} %fusion.4), kind=kLoop, calls=%fused_computation.1 | loop fusion | flops 12582912 | bytes 12582912 | tf_op jit(solution)/shard_map/concatenate | solution.py:34
  179.9 0.2 reduce-scatter.7.cloned.1.call-start
  180.2 8.0 %convolution_convert_fusion.1 = bf16[2048,1024]{0,1:T(8,128)(2,1)} fusion(bf16[768,1024]{1,0:T(8,128)(2,1)} %copy-done.6, bf16[2304,2048]{1,0:T(8,128)(2,1)} %all-gather.3.cloned.1.call-done), kind=kOutput, calls=%fused_computation.3 | convolution fusion | flops 3223322624 | bytes 8912896 | tf_op jit(solution)/shard_map/dot_general | solution.py:76
  188.2 7.3 %convolution_convert_fusion = bf16[2048,1024]{0,1:T(8,128)(2,1)} fusion(bf16[2304,2048]{1,0:T(8,128)(2,1)} %all-gather.3.cloned.1.call-done, f32[768,1024]{1,0:T(8,128)S(1)} %copy-done.5), kind=kOutput, calls=%fused_computation.2 | convolution fusion | flops 3225681920 | bytes 10485760 | tf_op jit(solution)/shard_map/dot_general | solution.py:79
  195.4 8.5 %pad_maximum_fusion = bf16[2048,2048]{0,1:T(8,128)(2,1)} fusion(bf16[2048,1024]{0,1:T(8,128)(2,1)} %convolution_convert_fusion, bf16[2048,1024]{0,1:T(8,128)(2,1)} %convolution_convert_fusion.1), kind=kLoop, calls=%fused_computation | loop fusion | flops 16777216 | bytes 16777216 | tf_op jit(solution)/shard_map/concatenate | solution.py:74
  204.0 12.3 %copy.22 = bf16[2048,2048]{1,0:T(8,128)(2,1)} copy(bf16[2048,2048]{0,1:T(8,128)(2,1)} %pad_maximum_fusion) | data formatting | bytes 16777216
  216.3 1.0 copy-done
  217.7 5.9 %reduce-scatter.5.cloned.1.call-done = bf16[1536,256]{1,0:T(8,128)(2,1)} async-done(((bf16[1536,2048]{1,0:T(8,128)(2,1)}), bf16[1536,256]{1,0:T(8,128)(2,1)}) %reduce-scatter.5.cloned.1.call-update) | async-done | bytes 786448 | tf_op jit(solution)/shard_map/reduce_scatter | solution.py:35
  223.6 2.0 fusion.27
  225.6 87.0 %reduce-scatter.7.cloned.1.call-done = bf16[128,2048]{1,0:T(8,128)(2,1)} async-done(((bf16[2048,2048]{1,0:T(8,128)(2,1)}), bf16[128,2048]{1,0:T(8,128)(2,1)}) %reduce-scatter.7.cloned.1.call-update) | async-done | bytes 524304
  312.6 1.3 copy.23
  314.1 1.0 copy.20
  315.1 1.0 copy.21
  (23 shorter events, 0.8 us)
Async XLA Ops:
  7.2 83.4 %all-gather.5.cloned.1.call-start = ((), (), s32[]{:S(2)}) async-start(), calls=%async_computation.3 | async-start | bytes 8912896 | tf_op jit(solution)/shard_map/all_gather | solution.py:23
  10.1 139.9 %all-gather.3.cloned.1.call-start = ((), (), s32[]{:S(2)}) async-start(), calls=%async_computation.2 | async-start | bytes 10616832 | tf_op jit(solution)/shard_map/all_gather | solution.py:16
  12.5 211.0 %reduce-scatter.5.cloned.1.call-start = ((), (), s32[]{:S(2)}) async-start(), calls=%async_computation.4 | async-start | bytes 7077888 | tf_op jit(solution)/shard_map/reduce_scatter | solution.py:35
  150.0 6.4 %copy-start.2 = (bf16[2304,2048]{1,0:T(8,128)(2,1)S(1)}, bf16[2304,2048]{1,0:T(8,128)(2,1)}, u32[]{:S(2)}) copy-start(bf16[2304,2048]{1,0:T(8,128)(2,1)} %all-gather.3.cloned.1.call-done) | copy-start | bytes 28311556
  150.0 8.2 %copy-start.3 = (bf16[2048,2048]{0,1:T(8,128)(2,1)S(1)}, bf16[2048,2048]{0,1:T(8,128)(2,1)}, u32[]{:S(2)}) copy-start(bf16[2048,2048]{0,1:T(8,128)(2,1)} %all-gather.5.cloned.1.call-done) | copy-start | bytes 25165828
  158.3 4.7 %copy-start.4 = (f32[768,1024]{1,0:T(8,128)}, f32[768,1024]{1,0:T(8,128)S(1)}, u32[]{:S(2)}) copy-start(f32[768,1024]{1,0:T(8,128)S(1)} %fusion.8) | copy-start | bytes 9437188
  166.5 3.7 %copy-start.6 = (bf16[768,1024]{1,0:T(8,128)(2,1)}, bf16[768,1024]{1,0:T(8,128)(2,1)S(1)}, u32[]{:S(2)}) copy-start(bf16[768,1024]{1,0:T(8,128)(2,1)S(1)} %multiply_convert_fusion.1) | copy-start | bytes 4718596
  179.9 8.2 %copy-start.5 = (f32[768,1024]{1,0:T(8,128)S(1)}, f32[768,1024]{1,0:T(8,128)}, u32[]{:S(2)}) copy-start(f32[768,1024]{1,0:T(8,128)} %copy-done.4) | copy-start | bytes 9437188
  179.9 132.7 %reduce-scatter.7.cloned.1.call-start = ((), (), s32[]{:S(2)}) async-start(), calls=%async_computation.5 | async-start | bytes 8912896
  216.2 1.0 copy-start
  216.2 1.2 copy-start.1
Sparse Core Ops, SparseCore 0:
  10.7 79.8 all-gather.4
  92.8 57.2 all-gather.2
  180.0 43.4 reduce-scatter.4
  226.8 85.7 reduce-scatter.6
where the time goes:
time: 323 us
  waiting for transfers between devices  230 us (71%)
  matrix products  39.4 us (12%)
  local copies, waits for them, and re-layouts  22 us (7%)
  other arithmetic  16.6 us (5%)
  between operations  13.9 us (4%)
    unnamed x5, waiting for transfers between devices  87.1 us
    all_gather x1, waiting for transfers between devices, gather_turned(): filled = lax.all_gather(both, axis, axis=0, tiled=True)  77.9 us
    all_gather x1, waiting for transfers between devices, in_one_piece(): lax.all_gather(both, axis, axis=dim, tiled=True)  59.5 us
    unnamed x21, local copies, waits for them, and re-layouts  20 us
    concatenate x1, other arithmetic, on_device(): jnp.concatenate((lax.dot_general(earlier_full, up_grad, contract_first, p...  8.54 us
    dot_general x1, matrix products, on_device(): lax.dot_general(earlier_full, up_grad, contract_first, preferred_element_...  8 us
    dot_general x1, matrix products, on_device(): lax.dot_general(cot_full, earlier_hidden, contract_first, preferred_eleme...  7.27 us
  transfers between devices with their start and end apart: 4, of which 4 were waited for; matrix products, arithmetic and copies ran while one was open for 13% of the time, Pallas kernels for 0%

commit v1 on v0

--- a/solution.py
+++ b/solution.py
@@ -20,7 +20,10 @@
     turned = [jnp.moveaxis(a, dim, 0) for a, dim in zip(arrays, dims)]
     widths = [t[0].size for t in turned]
     both = jnp.concatenate([t.reshape(-1, w) for t, w in zip(turned, widths)], axis=1)
-    filled = lax.all_gather(both, axis, axis=0, tiled=True)
+    size = lax.axis_size(axis)
+    parts = jnp.stack([both for _ in range(size)])
+    parts = lax.all_to_all(parts, axis, split_axis=0, concat_axis=0)
+    filled = jnp.concatenate(parts, axis=0)
     tiles = jnp.split(filled, [sum(widths[:k]) for k in range(1, len(widths))], axis=1)
     return tuple(
         (

time: 323 us -> 285 us (0.88)
  waiting for transfers between devices: 230 us -> 89.8 us
  blocking collectives: 0 us -> 104 us
    all_to_all x0 -> x1, blocking collectives: none -> 104 us  [gather_turned(): parts = lax.all_to_all(parts, axis, split_axis=0, concat_axis=0)]
    all_gather x1 -> x0, waiting for transfers between devices: 77.9 us -> none  [gather_turned(): filled = lax.all_gather(both, axis, axis=0, tiled=True)]
    all_gather x1, waiting for transfers between devices: 59.5 us -> 0.01 us  [in_one_piece(): lax.all_gather(both, axis, axis=dim, tiled=True)]
    unnamed x21 -> x25, local copies, waits for them, and re-layouts: 20 us -> 21.5 us
    unnamed x5 -> x4, waiting for transfers between devices: 87.1 us -> 87.1 us
  transfers between devices with their start and end apart: 4 -> 3, of which waited for: 4 -> 2; matrix products, arithmetic and copies ran while one was open for 13% -> 14% of each run, Pallas kernels for 0% -> 0%
where the time goes in v1:
time: 285 us; the launch traced here: 284 us
  blocking collectives  104 us (36%)
  waiting for transfers between devices  89.8 us (32%)
  matrix products  36.7 us (13%)
  local copies, waits for them, and re-layouts  24.8 us (9%)
  other arithmetic  14.9 us (5%)
  between operations  13.9 us (5%)
    all_to_all x1, blocking collectives, gather_turned(): parts = lax.all_to_all(parts, axis, split_axis=0, concat_axis=0)  104 us
    unnamed x4, waiting for transfers between devices  87.1 us
    unnamed x25, local copies, waits for them, and re-layouts  21.5 us
    concatenate x1, other arithmetic, on_device(): jnp.concatenate((lax.dot_general(earlier_full, up_grad, contract_first, p...  8.55 us
    dot_general x1, matrix products, on_device(): lax.dot_general(earlier_full, up_grad, contract_first, preferred_element_...  8 us
    dot_general x1, matrix products, on_device(): lax.dot_general(cot_full, earlier_hidden, contract_first, preferred_eleme...  6.95 us
    dot_general x1, matrix products, on_device(): jnp.dot(earlier_full, up_whole, preferred_element_type=jnp.float32)  6.3 us
  transfers between devices with their start and end apart: 3, of which 2 were waited for; matrix products, arithmetic and copies ran while one was open for 14% of the time, Pallas kernels for 0%

profile of v1, /device:TPU:0, one launch (start us, length us, event | category | flops | bytes accessed | tf_op | source)
XLA Modules:
  0.0 284.2 jit_solution(4400937559740373198)
XLA Ops:
  7.2 2.4 pad_maximum_fusion.2
  10.1 1.1 stack.2
  11.2 103.7 %all_to_all.5 = bf16[16,128,2048]{2,1,0:T(8,128)(2,1)} all-to-all(bf16[16,128,2048]{2,1,0:T(8,128)(2,1)S(1)} %stack.2), channel_id=1, replica_groups=mesh['fs'=16,'tp'=8] {'fs'}, dimensions={0} | all-to-all | bytes 16777216 | tf_op jit(solution)/shard_map/all_to_all | solution.py:25
  114.9 6.3 %fusion.8 = f32[768,1024]{1,0:T(8,128)S(1)} fusion(bf16[2048,2048]{1,0:T(8,128)(2,1)} %bitcast.5, bf16[2304,2048]{1,0:T(8,128)(2,1)} %all-gather.2.cloned.1.call-done), kind=kOutput, calls=%fused_computation.11 | convolution fusion | flops 3221225472 | bytes 10485760 | tf_op jit(solution)/shard_map/dot_general | solution.py:56
  121.2 1.8 copy-done.6
  123.0 1.3 copy-done.5
  124.3 3.5 %multiply_convert_fusion.1 = bf16[768,1024]{1,0:T(8,128)(2,1)S(1)} fusion(f32[768,1024]{1,0:T(8,128)S(1)} %fusion.8, bf16[2048,2048]{1,0:T(8,128)(2,1)S(1)} %bitcast.6, bf16[2304,2048]{1,0:T(8,128)(2,1)S(1)} %copy-done.5), kind=kOutput, calls=%fused_computation.17 | convolution fusion | flops 3224371200 | bytes 12058624 | tf_op jit(solution)/shard_map/dot_general | solution.py:59
  127.8 1.1 copy-done.8
  128.9 3.7 %convolution_convert_fusion.2 = bf16[768,2048]{1,0:T(8,128)(2,1)S(1)} fusion(bf16[768,1024]{1,0:T(8,128)(2,1)S(1)} %multiply_convert_fusion.1, bf16[2048,2048]{1,0:T(8,128)(2,1)S(1)} %bitcast.7), kind=kOutput, calls=%fused_computation.9 | convolution fusion | flops 3222798336 | bytes 8912896 | tf_op jit(solution)/shard_map/dot_general | solution.py:63
  132.6 4.6 %fusion.28 = (bf16[768,1024]{1,0:T(8,128)(2,1)}, f32[768,1024]{1,0:T(8,128)S(1)}) fusion(bf16[2048,2048]{1,0:T(8,128)(2,1)S(1)} %bitcast.8, bf16[2304,2048]{1,0:T(8,128)(2,1)S(1)} %copy-done.5), kind=kOutput, calls=%fused_computation.34 | convolution fusion | flops 3222011904 | bytes 12058624 | tf_op jit(solution)/shard_map/dot_general | solution.py:55
  137.2 3.7 %fusion.4 = bf16[768,2048]{1,0:T(8,128)(2,1)S(1)} fusion(bf16[2048,2048]{1,0:T(8,128)(2,1)S(1)} %bitcast.9, f32[768,1024]{1,0:T(8,128)S(1)} %get-tuple-element.20), kind=kOutput, calls=%fused_computation.8 | convolution fusion | flops 3225157632 | bytes 10485760 | tf_op jit(solution)/shard_map/dot_general | solution.py:58
  140.9 3.8 %pad_maximum_fusion.1 = bf16[1536,2048]{1,0:T(8,128)(2,1)} fusion(bf16[768,2048]{1,0:T(8,128)(2,1)S(1)} %convolution_convert_fusion.2, bf16[768,2048]{1,0:T(8,128)(2,1)S(1)} %fusion.4), kind=kLoop, calls=%fused_computation.1 | loop fusion | flops 12582912 | bytes 12582912 | tf_op jit(solution)/shard_map/concatenate | solution.py:37
  144.8 0.2 reduce-scatter.7.cloned.1.call-start
  145.0 8.0 %convolution_convert_fusion.1 = bf16[2048,1024]{0,1:T(8,128)(2,1)} fusion(bf16[768,1024]{1,0:T(8,128)(2,1)} %copy-done.8, bf16[2304,2048]{1,0:T(8,128)(2,1)} %all-gather.2.cloned.1.call-done), kind=kOutput, calls=%fused_computation.3 | convolution fusion | flops 3223322624 | bytes 8912896 | tf_op jit(solution)/shard_map/dot_general | solution.py:79
  153.0 7.0 %convolution_convert_fusion = bf16[2048,1024]{0,1:T(8,128)(2,1)} fusion(bf16[2304,2048]{1,0:T(8,128)(2,1)} %all-gather.2.cloned.1.call-done, f32[768,1024]{1,0:T(8,128)S(1)} %copy-done.7), kind=kOutput, calls=%fused_computation.2 | convolution fusion | flops 3225681920 | bytes 10485760 | tf_op jit(solution)/shard_map/dot_general | solution.py:82
  160.0 8.6 %pad_maximum_fusion = bf16[2048,2048]{0,1:T(8,128)(2,1)} fusion(bf16[2048,1024]{0,1:T(8,128)(2,1)} %convolution_convert_fusion, bf16[2048,1024]{0,1:T(8,128)(2,1)} %convolution_convert_fusion.1), kind=kLoop, calls=%fused_computation | loop fusion | flops 16777216 | bytes 16777216 | tf_op jit(solution)/shard_map/concatenate | solution.py:77
  168.5 12.4 %copy.24 = bf16[2048,2048]{1,0:T(8,128)(2,1)} copy(bf16[2048,2048]{0,1:T(8,128)(2,1)} %pad_maximum_fusion) | data formatting | bytes 16777216
  181.0 1.0 copy-done.1
  182.4 2.7 reduce-scatter.5.cloned.1.call-done
  185.1 2.0 fusion.27
  187.1 87.1 %reduce-scatter.7.cloned.1.call-done = bf16[128,2048]{1,0:T(8,128)(2,1)} async-done(((bf16[2048,2048]{1,0:T(8,128)(2,1)}), bf16[128,2048]{1,0:T(8,128)(2,1)}) %reduce-scatter.7.cloned.1.call-update) | async-done | bytes 524304
  274.2 1.3 copy.25
  275.7 1.0 copy.22
  276.7 1.0 copy.23
  (27 shorter events, 1.1 us)
Async XLA Ops:
  7.2 2.5 copy-start.3
  7.2 2.7 copy-start.4
  7.2 107.7 %all-gather.2.cloned.1.call-start = ((), (), s32[]{:S(2)}) async-start(), calls=%async_computation.3 | async-start | bytes 10616832 | tf_op jit(solution)/shard_map/all_gather | solution.py:16
  9.6 175.4 %reduce-scatter.5.cloned.1.call-start = ((), (), s32[]{:S(2)}) async-start(), calls=%async_computation.4 | async-start | bytes 7077888 | tf_op jit(solution)/shard_map/reduce_scatter | solution.py:38
  114.9 8.1 %copy-start = (bf16[16,128,2048]{2,1,0:T(8,128)(2,1)S(1)}, bf16[16,128,2048]{2,1,0:T(8,128)(2,1)}, u32[]{:S(2)}) copy-start(bf16[16,128,2048]{2,1,0:T(8,128)(2,1)} %all_to_all.5) | copy-start | bytes 25165828
  114.9 9.4 %copy-start.5 = (bf16[2304,2048]{1,0:T(8,128)(2,1)S(1)}, bf16[2304,2048]{1,0:T(8,128)(2,1)}, u32[]{:S(2)}) copy-start(bf16[2304,2048]{1,0:T(8,128)(2,1)} %all-gather.2.cloned.1.call-done) | copy-start | bytes 28311556
  121.2 1.8 copy-start.6
  127.8 1.1 copy-start.8
  144.8 8.2 %copy-start.7 = (f32[768,1024]{1,0:T(8,128)S(1)}, f32[768,1024]{1,0:T(8,128)}, u32[]{:S(2)}) copy-start(f32[768,1024]{1,0:T(8,128)} %copy-done.6) | copy-start | bytes 9437188
  144.8 129.4 %reduce-scatter.7.cloned.1.call-start = ((), (), s32[]{:S(2)}) async-start(), calls=%async_computation.5 | async-start | bytes 8912896
  180.9 1.1 copy-start.1
  180.9 1.2 copy-start.2
Sparse Core Ops, SparseCore 0:
  10.2 60.4 all-gather.1
  144.9 40.1 reduce-scatter.4
  188.5 85.6 reduce-scatter.6
